TPU v7x, 32 devices: a whole 2x2x4 slice. The times are simulated.
32 devices in a mesh: sp: 16 (over z, y, x), tp: 2 (over core).
Axes of the slice: x: 2, y: 2, z: 4, core: 2. Of those that a mesh axis runs over, the one named last changes fastest.
Arguments:
- query_heads: bfloat16 [2048, 1024], P('sp', 'tp'), may hold values from -12 to 12
- key_heads: bfloat16 [2048, 1024], P('sp', 'tp'), may hold values from -6 to 6
- value_heads: bfloat16 [2048, 1024], P('sp', 'tp'), may hold values from -6 to 6
- decay_sums: float32 [2048, 8], P('sp', 'tp'), may hold values from -338 to 0, as said below
- row_logsums: float32 [2048, 8], P('sp', 'tp'), may hold values from -9216 to 11264
- head_outputs: bfloat16 [2048, 1024], P('sp', 'tp'), may hold values from -1.796875 to 1.796875
- out_cotangent: bfloat16 [2048, 1024], P('sp', 'tp'), may hold values from -24 to 24
- normed_input: bfloat16 [2048, 2048], P('sp', 'tp'), may hold values from -6 to 6
Outputs:
- query_grads: bfloat16 [2048, 1024], P('sp', 'tp')
- key_grads: bfloat16 [2048, 1024], P('sp', 'tp')
- value_grads: bfloat16 [2048, 1024], P('sp', 'tp')
- weight_grad: float32 [2048, 1024], P('sp', 'tp')
Inputs may be any that keep to these rules, and one draw needn't show every extreme that they name: `decay_sums`: each head's values never rise along the positions.
All inputs are finite; a program needn't handle non-finite values.
Results may differ from a plain program's by a relative error of at most 0.005.
Values may be sent and summed in bfloat16 or wider, within the bound.
A program may use at most 64 MiB of HBM per device.

v0:
```python
import jax
import jax.numpy as jnp
from jax import lax
from jax.sharding import PartitionSpec as P


def block_length(whole_rows):
    length = whole_rows
    while length > 1024 and length % 2 == 0:
        length = length // 2
    return length


def split_heads(block, head_count):
    return block.reshape(block.shape[0], head_count, block.shape[1] // head_count)


def attention_weights(
    query_part, key_part, norm_part, gate_query, gate_key, query_pos, key_pos, score_scale
):
    scores = (
        jnp.einsum("ahd,bhd->hab", query_part, key_part, preferred_element_type=jnp.float32)
        * score_scale
    )
    scores = scores + (gate_query.T[:, :, None] - gate_key.T[:, None, :])
    allowed = key_pos[None, None, :] <= query_pos[None, :, None]
    return jnp.exp(jnp.where(allowed, scores - norm_part.T[:, :, None], -jnp.inf))


def score_slopes(weights, grad_part, value_part, term_part):
    flows = jnp.einsum("ahd,bhd->hab", grad_part, value_part, preferred_element_type=jnp.float32)
    return weights * (flows - term_part.T[:, :, None])


def over_blocks(visit_block, running, members):
    whole_rows = members[0].shape[0]
    length = block_length(whole_rows)
    number = whole_rows // length
    stacked = tuple((member.reshape((number, length) + member.shape[1:]) for member in members))

    def visit_one(carried, scanned):
        block_index, block_parts = scanned
        token_places = block_index * length + jnp.arange(length, dtype=jnp.int32)
        return (visit_block(carried, block_parts, token_places), None)

    result, unused = lax.scan(visit_one, running, (jnp.arange(number, dtype=jnp.int32), stacked))
    return result


def per_device(
    query_heads,
    key_heads,
    value_heads,
    decay_sums,
    row_logsums,
    head_outputs,
    out_cotangent,
    normed_input,
):
    own_rows, row_width = query_heads.shape
    head_count = decay_sums.shape[1]
    score_scale = (row_width // head_count) ** (-0.5)
    own_pos = lax.axis_index("sp") * own_rows + jnp.arange(own_rows, dtype=jnp.int32)
    own_query = split_heads(query_heads, head_count)
    own_key = split_heads(key_heads, head_count)
    own_value = split_heads(value_heads, head_count)
    own_grad = split_heads(out_cotangent, head_count)
    row_terms = jnp.einsum(
        "ahd,ahd->ah",
        split_heads(head_outputs, head_count),
        own_grad,
        preferred_element_type=jnp.float32,
    )
    all_gates, all_logsums, all_terms = (
        lax.all_gather(decay_sums, "sp", axis=0, tiled=True),
        lax.all_gather(row_logsums, "sp", axis=0, tiled=True),
        lax.all_gather(row_terms, "sp", axis=0, tiled=True),
    )

    def query_side(query_sum, key_part, value_part, key_pos):
        gate_key = lax.dynamic_slice_in_dim(all_gates, key_pos[0], key_pos.shape[0], 0)

        def query_compute(running):
            weights = attention_weights(
                own_query,
                key_part,
                row_logsums,
                decay_sums,
                gate_key,
                own_pos,
                key_pos,
                score_scale,
            )
            slopes = score_slopes(weights, own_grad, value_part, row_terms)
            return running + jnp.einsum(
                "hab,bhd->ahd",
                slopes.astype(jnp.bfloat16),
                key_part,
                preferred_element_type=jnp.float32,
            )

        return lax.cond(
            key_pos[0] <= own_pos[-1], query_compute, lambda running: running, query_sum
        )

    def key_side(key_sums, query_part, grad_part, query_pos):
        length = query_pos.shape[0]
        gate_query = lax.dynamic_slice_in_dim(all_gates, query_pos[0], length, 0)
        norm_part = lax.dynamic_slice_in_dim(all_logsums, query_pos[0], length, 0)
        term_part = lax.dynamic_slice_in_dim(all_terms, query_pos[0], length, 0)

        def key_compute(running):
            key_sum, value_sum = running
            weights = attention_weights(
                query_part,
                own_key,
                norm_part,
                gate_query,
                decay_sums,
                query_pos,
                own_pos,
                score_scale,
            )
            slopes = score_slopes(weights, grad_part, own_value, term_part)
            key_sum = key_sum + jnp.einsum(
                "hab,ahd->bhd",
                slopes.astype(jnp.bfloat16),
                query_part,
                preferred_element_type=jnp.float32,
            )
            value_sum = value_sum + jnp.einsum(
                "hab,ahd->bhd",
                weights.astype(jnp.bfloat16),
                grad_part,
                preferred_element_type=jnp.float32,
            )
            return (key_sum, value_sum)

        return lax.cond(query_pos[-1] >= own_pos[0], key_compute, lambda running: running, key_sums)

    zero_sums = jnp.zeros((own_rows, head_count, row_width // head_count), jnp.float32)

    def visit_block(carried, block_parts, token_places):
        return query_side(
            carried,
            split_heads(block_parts[0], head_count),
            split_heads(block_parts[1], head_count),
            token_places,
        )

    query_sum = over_blocks(
        visit_block,
        zero_sums,
        (
            lax.all_gather(key_heads, "sp", axis=0, tiled=True),
            lax.all_gather(value_heads, "sp", axis=0, tiled=True),
        ),
    )

    def visit_block(carried, block_parts, token_places):
        return key_side(
            carried,
            split_heads(block_parts[0], head_count),
            split_heads(block_parts[1], head_count),
            token_places,
        )

    key_sum, value_sum = over_blocks(
        visit_block,
        (zero_sums, zero_sums),
        (
            lax.all_gather(query_heads, "sp", axis=0, tiled=True),
            lax.all_gather(out_cotangent, "sp", axis=0, tiled=True),
        ),
    )
    query_grads = (query_sum * score_scale).astype(jnp.bfloat16).reshape(own_rows, row_width)
    key_grads = (key_sum * score_scale).astype(jnp.bfloat16).reshape(own_rows, row_width)
    value_grads = value_sum.astype(jnp.bfloat16).reshape(own_rows, row_width)
    whole_input = lax.all_gather(normed_input, "tp", axis=1, tiled=True)
    own_features = lax.all_to_all(whole_input, "sp", split_axis=1, concat_axis=0, tiled=True)
    weight_grad = lax.dot_general(
        own_features,
        lax.all_gather(query_grads, "sp", axis=0, tiled=True),
        (((0,), (0,)), ((), ())),
        preferred_element_type=jnp.float32,
    )
    return (query_grads, key_grads, value_grads, weight_grad)


def solution(mesh):
    return jax.shard_map(
        per_device,
        mesh=mesh,
        in_specs=(
            P("sp", "tp"),
            P("sp", "tp"),
            P("sp", "tp"),
            P("sp", "tp"),
            P("sp", "tp"),
            P("sp", "tp"),
            P("sp", "tp"),
            P("sp", "tp"),
        ),
        out_specs=(P("sp", "tp"), P("sp", "tp"), P("sp", "tp"), P("sp", "tp")),
        check_vma=False,
    )
```

profile of v0, /device:TPU:8, one launch (start us, length us, event | category | flops | bytes accessed | tf_op | source)
XLA Modules:
  0.0 339.3 jit_solution(5487230171018308837)
XLA Ops:
  14.1 37.5 %all_gather.28 = f32[2048,4]{0,1:T(4,128)} all-gather(f32[128,4]{0,1:T(4,128)} %param.19), channel_id=1, replica_groups=mesh['sp'=16,'tp'=2] {'sp'}, dimensions={0}, use_global_device_ids=true | all-gather | bytes 34816 | tf_op jit(solution)/shard_map/all_gather | solution.py:75
  52.1 20.3 %all-gather.6.cloned.1.call-done = bf16[2048,512]{1,0:T(8,128)(2,1)} async-done(((bf16[128,512]{1,0:T(8,128)(2,1)}), bf16[2048,512]{1,0:T(8,128)(2,1)}) %all-gather.6.cloned.1.call-update) | async-done | bytes 2097168 | tf_op jit(solution)/shard_map/all_gather | solution.py:155
  72.4 3.9 %copy.89 = bf16[2,1024,512]{1,2,0:T(8,128)(2,1)} copy(bf16[2,1024,512]{2,1,0:T(8,128)(2,1)} %bitcast.124) | data formatting | bytes 4194304 | tf_op jit(solution)/shard_map/while | solution.py:46
  76.3 58.0 %all-gather.8.cloned.1.call-done = bf16[2048,512]{1,0:T(8,128)(2,1)} async-done(((bf16[128,512]{1,0:T(8,128)(2,1)}), bf16[2048,512]{1,0:T(8,128)(2,1)}) %all-gather.8.cloned.1.call-update) | async-done | bytes 2097168 | tf_op jit(solution)/shard_map/all_gather | solution.py:156
  134.4 4.0 %copy.91 = bf16[2,1024,512]{1,2,0:T(8,128)(2,1)} copy(bf16[2,1024,512]{2,1,0:T(8,128)(2,1)} %bitcast.125) | data formatting | bytes 4194304 | tf_op jit(solution)/shard_map/while | solution.py:46
  139.1 19.1 %while.25 = (s32[]{:T(128)}, f32[128,4,128]{2,0,1:T(8,128)}, s32[2]{0:T(128)S(1)}, s32[128]{0:T(128)}, bf16[2,1024,512]{1,2,0:T(8,128)(2,1)}, /*index=5*/bf16[12...) while((s32[]{:T(128)}, f32[128,4,128]{2,0,1:T(8,128)}, ...), condition=%wide.region_3.4_spmd, body=%wide.region_0.3_spmd.sunk | while | flops 407045120 | bytes 12647265 | solution.py:46
  140.9 1.2 slice.24
  143.4 10.4 %conditional.4 = (f32[128,4,128]{2,0,1:T(8,128)}) conditional(s32[]{:T(128)} %convert_element_type.67, f32[128,4,128]{2,0,1:T(8,128)} %get-tuple-element.798, (s32[1024]{0:T(1024)S(1)}, s32[128]{0:T(128)}, bf16[2,1024,512]{1,2,0:T(8,128)(2,1)}, s32[]{:T(128)}, bf16[128,4,128]{2,0,1:T(8,128)(2,1)S(1)}, /*index=5*/f32[128,4]{0,1:T(4,128)}, s32[]{:T(128)}, ...), branch_computations={%region_1.1_spmd, %region_2.2_spmd} | conditional | flops 407044096 | bytes 12642866 | solution.py:102
  143.4 2.8 constant_dynamic-slice_fusion
  150.3 3.6 %fusion.6 = f32[128,4,128]{2,0,1:T(8,128)} fusion(f32[128,4,128]{2,0,1:T(8,128)} %get-tuple-element.392, bf16[1024,4,128]{0,2,1:T(8,128)(2,1)S(1)} %bitcast.120, f32[4,1024,128]{2,1,0:T(8,128)S(1)} %fusion.24, bf16[1024,4,128]{0,2,1:T(8,128)(2,1)} %bitcast.121, bf16[128,4,128]{2,0,1:T(8,128)(2,1)} %get-tuple-element.403, f32[4,128]{1,0:T(4,128)S(1)} %bitcast.134, ...), kind=kOutput, calls=%fused_computation.8 | convolution fusion | flops 272695296 | bytes 5003264 | tf_op jit(solution)/shard_map/while/body/eval_jaxpr/cond/branch_1_fun/hab,bhd->ahd/dot_general | solution.py:95
  155.7 1.2 slice.24
  158.2 1.7 copy_bitcast_fusion.2
  159.9 1.1 copy.102
  161.0 2.3 all_gather.35
  163.4 15.2 %all-to-all-start = ((bf16[128,16,128]{0,2,1:T(8,128)(2,1)}), bf16[128,16,128]{0,2,1:T(8,128)(2,1)S(1)}, u32[]{:S(2)}, u32[]{:S(2)}) async-start(bf16[128,16,128]{0,2,1:T(8,128)(2,1)} %bitcast.31), calls=%async_computation | async-start | bytes 1048576 | tf_op jit(solution)/shard_map/all_to_all | solution.py:180
  179.7 47.5 %all_gather.31 = f32[2048,4]{0,1:T(4,128)} all-gather(f32[128,4]{0,1:T(4,128)S(1)} %get-tuple-element.895), channel_id=1, replica_groups=mesh['sp'=16,'tp'=2] {'sp'}, dimensions={0}, use_global_device_ids=true | all-gather | bytes 34816 | tf_op jit(solution)/shard_map/all_gather | solution.py:76
  227.2 38.3 %all_gather.33 = f32[2048,4]{0,1:T(4,128)} all-gather(f32[128,4]{0,1:T(4,128)S(1)} %get-tuple-element.894), channel_id=1, replica_groups=mesh['sp'=16,'tp'=2] {'sp'}, dimensions={0}, use_global_device_ids=true | all-gather | bytes 34816 | tf_op jit(solution)/shard_map/all_gather | solution.py:77
  266.6 4.0 %copy.96 = bf16[2,1024,512]{1,2,0:T(8,128)(2,1)} copy(bf16[2,1024,512]{2,1,0:T(8,128)(2,1)} %bitcast.122) | data formatting | bytes 4194304 | tf_op jit(solution)/shard_map/while | solution.py:46
  270.6 4.0 %copy.98 = bf16[2,1024,512]{1,2,0:T(8,128)(2,1)} copy(bf16[2,1024,512]{2,1,0:T(8,128)(2,1)} %bitcast.123) | data formatting | bytes 4194304 | tf_op jit(solution)/shard_map/while | solution.py:46
  275.9 36.6 %while.26 = (s32[]{:T(128)}, f32[128,4,128]{2,0,1:T(8,128)}, f32[128,4,128]{2,0,1:T(8,128)S(1)}, s32[2]{0:T(128)}, s32[128]{0:T(128)}, /*index=5*/bf16[2,1024,51...) while((s32[]{:T(128)}, f32[128,4,128]{2,0,1:T(8,128)}, ...), condition=%wide.region_7.8_spmd, body=%wide.region_4.7_spmd.sunk | while | flops 541852672 | bytes 16411533 | solution.py:46
  275.9 1.2 dynamic_slice.93
  279.4 14.8 %conditional.5 = ((f32[128,4,128]{2,0,1:T(8,128)}, f32[128,4,128]{2,0,1:T(8,128)S(1)})) conditional(s32[]{:T(128)} %bitcast.114, (f32[128,4,128]{2,0,1:T(8,128)}, f32[128,4,128]{2,0,1:T(8,128)S(1)}) %tuple.87, (s32[128]{0:T(128)}, s32[1024]{0:T(1024)S(1)}, bf16[2,1024,512]{1,2,0:T(8,128)(2,1)}, s32[]{:T(128)}, bf16[128,4,128]{2,0,1:T(8,128)(2,1)}, ...), branch_computations={%region_5.5_spmd, %region_6.6_spmd} | conditional | flops 541851648 | bytes 16407118 | solution.py:139
  279.4 2.7 constant_dynamic-slice_fusion.2
  286.9 3.4 select_exponential_fusion
  290.3 3.3 fusion.18
  294.2 1.2 dynamic_slice.93
  297.6 14.8 %conditional.5 = ((f32[128,4,128]{2,0,1:T(8,128)}, f32[128,4,128]{2,0,1:T(8,128)S(1)})) conditional(s32[]{:T(128)} %bitcast.114, (f32[128,4,128]{2,0,1:T(8,128)}, f32[128,4,128]{2,0,1:T(8,128)S(1)}) %tuple.87, (s32[128]{0:T(128)}, s32[1024]{0:T(1024)S(1)}, bf16[2,1024,512]{1,2,0:T(8,128)(2,1)}, s32[]{:T(128)}, bf16[128,4,128]{2,0,1:T(8,128)(2,1)}, ...), branch_computations={%region_5.5_spmd, %region_6.6_spmd} | conditional | flops 541851648 | bytes 16407118 | solution.py:139
  297.7 2.7 constant_dynamic-slice_fusion.2
  305.2 3.4 select_exponential_fusion
  308.6 3.3 fusion.18
  314.8 14.7 %all-gather.14.cloned.1.call-done = bf16[2048,512]{1,0:T(8,128)(2,1)} async-done(((bf16[128,512]{1,0:T(8,128)(2,1)}), bf16[2048,512]{1,0:T(8,128)(2,1)}) %all-gather.14.cloned.1.call-update) | async-done | bytes 2097168 | tf_op jit(solution)/shard_map/all_gather | solution.py:183
  329.5 2.4 convolution_bitcast_fusion.1
  (65 shorter events, 27.5 us)
Async XLA Ops:
  7.2 65.2 %all-gather.6.cloned.1.call-start = ((), (), s32[]{:S(2)}) async-start(), calls=%async_computation.1 | async-start | bytes 2228224 | tf_op jit(solution)/shard_map/all_gather | solution.py:155
  7.9 126.5 %all-gather.8.cloned.1.call-start = ((), (), s32[]{:S(2)}) async-start(), calls=%async_computation.2 | async-start | bytes 2228224 | tf_op jit(solution)/shard_map/all_gather | solution.py:156
  8.6 258.0 %all-gather.10.cloned.1.call-start = ((), (), s32[]{:S(2)}) async-start(), calls=%async_computation.3 | async-start | bytes 2228224 | tf_op jit(solution)/shard_map/all_gather | solution.py:172
  9.4 261.2 %all-gather.12.cloned.1.call-start = ((), (), s32[]{:S(2)}) async-start(), calls=%async_computation.4 | async-start | bytes 2228224 | tf_op jit(solution)/shard_map/all_gather | solution.py:173
  10.0 319.6 %all-gather.14.cloned.1.call-start = ((), (), s32[]{:S(2)}) async-start(), calls=%async_computation.5 | async-start | bytes 2228224 | tf_op jit(solution)/shard_map/all_gather | solution.py:183
  134.4 4.7 %copy-start.2 = (f32[128,4]{0,1:T(4,128)S(1)}, f32[128,4]{0,1:T(4,128)}, u32[]{:S(2)}) copy-start(f32[128,4]{0,1:T(4,128)} %param.20) | copy-start | bytes 6148
  158.2 20.4 %copy-start = (bf16[128,512]{1,0:T(8,128)(2,1)S(1)}, bf16[128,512]{1,0:T(8,128)(2,1)}, u32[]{:S(2)}) copy-start(bf16[128,512]{1,0:T(8,128)(2,1)} %param.17) | copy-start | bytes 393220
  158.2 20.5 %copy-start.1 = (bf16[128,512]{1,0:T(8,128)(2,1)S(1)}, bf16[128,512]{1,0:T(8,128)(2,1)}, u32[]{:S(2)}) copy-start(bf16[128,512]{1,0:T(8,128)(2,1)} %param.18) | copy-start | bytes 393220
  163.4 102.2 %all-to-all-start = ((bf16[128,16,128]{0,2,1:T(8,128)(2,1)}), bf16[128,16,128]{0,2,1:T(8,128)(2,1)S(1)}, u32[]{:S(2)}, u32[]{:S(2)}) async-start(bf16[128,16,128]{0,2,1:T(8,128)(2,1)} %bitcast.31), calls=%async_computation | async-start | bytes 1048576 | tf_op jit(solution)/shard_map/all_to_all | solution.py:180
Sparse Core Ops, SparseCore 0:
  10.7 61.5 all-gather.5
  75.2 59.1 all-gather.7
  137.1 66.3 all-gather.9
  206.2 60.8 all-gather.11
  270.2 59.2 all-gather.13
where the time goes:
time: 342 us; the launch traced here: 339 us
  blocking collectives  126 us (37%)
  waiting for transfers between devices  95.7 us (28%)
  local copies, waits for them, and re-layouts  49.3 us (14%)
  matrix products  20.9 us (6%)
  starting transfers between devices  15.4 us (5%)
  between operations  13.9 us (4%)
  loops' own time  12.9 us (4%)
  other arithmetic  5.65 us (2%)
    all_gather x1, waiting for transfers between devices, per_device(): lax.all_gather(value_heads, 'sp', axis=0, tiled=True)  58 us
    all_gather x1, blocking collectives, per_device(): lax.all_gather(row_logsums, 'sp', axis=0, tiled=True)  47.5 us
    all_gather x1, blocking collectives, per_device(): lax.all_gather(row_terms, 'sp', axis=0, tiled=True)  38.3 us
    all_gather x1, blocking collectives, per_device(): lax.all_gather(decay_sums, 'sp', axis=0, tiled=True)  37.5 us
    all_gather x1, waiting for transfers between devices, per_device(): lax.all_gather(key_heads, 'sp', axis=0, tiled=True)  20.3 us
    while x8, local copies, waits for them, and re-layouts, over_blocks(): lax.scan(visit_one, running, (jnp.arange(number, dtype=jnp.int32), stacked))  17.7 us
    all_to_all x1, starting transfers between devices, per_device(): lax.all_to_all(whole_input, 'sp', split_axis=1, concat_axis=0, tiled=True)  15.2 us
    all_gather x1, waiting for transfers between devices, per_device(): lax.all_gather(query_grads, 'sp', axis=0, tiled=True)  14.7 us
  transfers between devices with their start and end apart: 6, of which 3 were waited for; matrix products, arithmetic and copies ran while one was open for 21% of the time, Pallas kernels for 0%

commit v1 on v0

--- a/solution.py
+++ b/solution.py
@@ -1,6 +1,10 @@
+import functools
+
 import jax
 import jax.numpy as jnp
 from jax import lax
+from jax.experimental import pallas as pl
+from jax.experimental.pallas import tpu as pltpu
 from jax.sharding import PartitionSpec as P
 
 
@@ -47,7 +51,7 @@
     return result
 
 
-def per_device(
+def gathered_device(
     query_heads,
     key_heads,
     value_heads,
@@ -187,7 +191,382 @@
     return (query_grads, key_grads, value_grads, weight_grad)
 
 
+F32 = jnp.float32
+BF16 = jnp.bfloat16
+
+
+def dot_last(a, b):
+    return lax.dot_general(a, b, (((1,), (1,)), ((), ())), preferred_element_type=F32)
+
+
+def dot_plain(a, b):
+    return lax.dot_general(a, b, (((1,), (0,)), ((), ())), preferred_element_type=F32)
+
+
+def dot_first(a, b):
+    return lax.dot_general(a, b, (((0,), (0,)), ((), ())), preferred_element_type=F32)
+
+
+def fused_kernel(
+    sp, tp, u, n, hd,
+    q_ref, k_ref, v_ref, g_ref, l_ref, o_ref, do_ref, x_ref,
+    dq_out, dk_out, dv_out, w_out,
+    kbuf, vbuf, qbuf, dobuf, sbuf, ssend, tmp, cols, xbuf, dqpair, dkv, acc, wsend, wrecv,
+    main_send, main_recv, stat_send, stat_recv, x_send, x_recv,
+    pair_send, pair_recv, out_send, out_recv, w_send, w_recv,
+):
+    r = sp // u
+    length = u * n
+    owners = sp // tp
+    fw = x_ref.shape[1] // owners
+    scale = hd ** (-0.5)
+    me, p = lax.axis_index("sp"), lax.axis_index("tp")
+    z, g = me // u, me % u
+
+    def lanes(index, width=hd):
+        return pl.ds(pl.multiple_of(index * width, width), width)
+
+    def rows(index):
+        return pl.ds(pl.multiple_of(index * n, n), n)
+
+    def remote(src, dst, send, recv, i, t):
+        return pltpu.make_async_remote_copy(
+            src_ref=src, dst_ref=dst, send_sem=send, recv_sem=recv,
+            device_id={"sp": i, "tp": t}, device_id_type=pl.DeviceIdType.MESH,
+        )
+
+    barrier = pltpu.get_barrier_semaphore()
+    for d in range(1, sp * tp):
+        other = lax.rem(me * tp + p + d, sp * tp)
+        pl.semaphore_signal(
+            barrier, inc=1, device_id={"sp": other // tp, "tp": other % tp},
+            device_id_type=pl.DeviceIdType.MESH,
+        )
+
+    lane = lax.broadcasted_iota(jnp.int32, (n, hd), 1)
+    terms = jnp.zeros((n, hd), F32)
+    for h in range(u):
+        part = slice(h * hd, (h + 1) * hd)
+        total = jnp.sum(
+            o_ref[:, part].astype(F32) * do_ref[:, part].astype(F32), axis=1, keepdims=True
+        )
+        terms = jnp.where(lane == h, total, terms)
+    tmp[0] = jnp.zeros((n, hd), F32)
+    tmp[1] = jnp.zeros((n, hd), F32)
+    tmp[0, :, 0:u] = g_ref[...]
+    tmp[1, :, 0:u] = g_ref[...] - l_ref[...]
+    flat = (tmp[0].T, tmp[1].T, terms.T)
+    for h in range(u):
+        for s in range(3):
+            ssend[h, s : s + 1, :] = flat[s][h : h + 1, :]
+    pl.semaphore_wait(barrier, sp * tp - 1)
+
+    def head_of(j):
+        return lax.rem(g + j, u)
+
+    def source_of(j):
+        return lax.rem(g + u - j, u)
+
+    pairs = ((k_ref, kbuf), (v_ref, vbuf), (q_ref, qbuf), (do_ref, dobuf))
+
+    def main_copy(a, k, j):
+        ref, buf = pairs[a]
+        layer = z + k if a < 2 else z - k
+        h = head_of(j)
+        return remote(
+            ref.at[:, lanes(h)], buf.at[z, rows(g), :],
+            main_send.at[a, k, j], main_recv.at[a, k, j], layer * u + h, p,
+        )
+
+    def own_copy(a):
+        ref, buf = pairs[a]
+        return pltpu.make_async_copy(
+            ref.at[:, lanes(g)], buf.at[z, rows(g), :], main_recv.at[a, 0, 0]
+        )
+
+    def wait_main(a, k, j):
+        ref, buf = pairs[a]
+        layer = z - k if a < 2 else z + k
+        here = buf.at[layer, rows(source_of(j)), :]
+        pltpu.make_async_copy(here, here, main_recv.at[a, k, j]).wait()
+
+    def stat_copy(d, j):
+        h = head_of(j)
+        return remote(
+            ssend.at[h], sbuf.at[me], stat_send.at[d + r - 1, j], stat_recv.at[d + r - 1, j],
+            (z + d) * u + h, p,
+        )
+
+    def wait_stat(d, j):
+        here = sbuf.at[(z - d) * u + source_of(j)]
+        pltpu.make_async_copy(here, here, stat_recv.at[d + r - 1, j]).wait()
+
+    def own_stat():
+        return pltpu.make_async_copy(ssend.at[g], sbuf.at[me], stat_recv.at[r - 1, 0])
+
+    def x_copy(j):
+        return remote(
+            x_ref, xbuf.at[rows(g), :], x_send.at[j], x_recv.at[j], z * u + head_of(j), p
+        )
+
+    def up(k):
+        return z + k < r
+
+    def down(k):
+        return z >= k
+
+    def each_send(act):
+        for j in range(1, u):
+            act(stat_copy(0, j))
+        for a in (2, 0, 3, 1):
+            for j in range(1, u):
+                act(main_copy(a, 0, j))
+        for k in range(1, r):
+            for reach, sign, members in ((up, 1, (0, 1)), (down, -1, (2, 3))):
+
+                @pl.when(reach(k))
+                def _(k=k, sign=sign, members=members):
+                    for j in range(u):
+                        act(stat_copy(sign * k, j))
+                    for a in members:
+                        for j in range(u):
+                            act(main_copy(a, k, j))
+
+        for j in range(1, u):
+            act(x_copy(j))
+
+    each_send(lambda copy: copy.start())
+    own_stat().start()
+    for a in range(4):
+        own_copy(a).start()
+    own_x = pltpu.make_async_copy(x_ref, xbuf.at[rows(g), :], x_recv.at[0])
+    own_x.start()
+
+    for j in range(u):
+        wait_stat(0, j)
+        for a in range(4):
+            wait_main(a, 0, j)
+    for b in range(u):
+        for s in range(3):
+            row = sbuf[z * u + b, s : s + 1, :]
+            cols[s, b * n : (b + 1) * n, :] = jnp.broadcast_to(row, (hd, n)).T
+
+    width = 2 * n if u % 2 == 0 else n
+    pieces = width // n
+
+    def stat_row(s, layer, c):
+        return jnp.concatenate(
+            [sbuf[layer * u + c * pieces + i, s : s + 1, :] for i in range(pieces)], axis=1
+        )
+
+    def wide(s, part):
+        return jnp.concatenate([cols[s, part, :]] * pieces, axis=1)
+
+    def query_tile(b, c, part, masked):
+        keys = slice(c * width, (c + 1) * width)
+        kk, vv = kbuf[b, keys, :], vbuf[b, keys, :]
+        scores = dot_last(qbuf[z, part, :], kk) * scale + (wide(1, part) - stat_row(0, b, c))
+        if masked:
+            t = lax.broadcasted_iota(jnp.int32, scores.shape, 0) + part.start
+            s = lax.broadcasted_iota(jnp.int32, scores.shape, 1) + c * width
+            scores = jnp.where(s <= t, scores, -jnp.inf)
+        slopes = jnp.exp(scores) * (dot_last(dobuf[z, part, :], vv) - wide(2, part))
+        acc[0, part, :] += dot_plain(slopes.astype(BF16), kk)
+
+    def key_tile(a, c, part, masked):
+        span = slice(c * width, (c + 1) * width)
+        qq, dd = qbuf[a, span, :], dobuf[a, span, :]
+        scores = dot_last(kbuf[z, part, :], qq) * scale + (stat_row(1, a, c) - wide(0, part))
+        if masked:
+            s = lax.broadcasted_iota(jnp.int32, scores.shape, 0) + part.start
+            t = lax.broadcasted_iota(jnp.int32, scores.shape, 1) + c * width
+            scores = jnp.where(s <= t, scores, -jnp.inf)
+        weights = jnp.exp(scores)
+        slopes = weights * (dot_last(vbuf[z, part, :], dd) - stat_row(2, a, c))
+        acc[1, part, :] += dot_plain(slopes.astype(BF16), qq)
+        acc[2, part, :] += dot_plain(weights.astype(BF16), dd)
+
+    acc[...] = jnp.zeros_like(acc)
+    chunks = length // width
+    for c in range(chunks):
+        query_tile(z, c, slice(c * width, length), True)
+
+    @pl.loop(1, z + 1)
+    def _(k):
+        for j in range(u):
+            wait_stat(k, j)
+            wait_main(0, k, j)
+            wait_main(1, k, j)
+        for c in range(chunks):
+            query_tile(z - k, c, slice(0, length), False)
+
+    dqpair[p] = (acc[0] * scale).astype(BF16)
+    for j in range(u):
+        here = xbuf.at[rows(source_of(j)), :]
+        pltpu.make_async_copy(here, here, x_recv.at[j]).wait()
+
+    def pair_copy(j):
+        return remote(
+            dqpair.at[p], dqpair.at[p], pair_send.at[j], pair_recv.at[j], me, lax.rem(p + j, tp)
+        )
+
+    for j in range(1, tp):
+        pair_copy(j).start()
+
+    outs = (dq_out, dk_out, dv_out)
+
+    def out_source(m, h):
+        return dqpair.at[p, rows(h), :] if m == 0 else dkv.at[m - 1, rows(h), :]
+
+    def out_copy(m, j):
+        h = head_of(j)
+        return remote(
+            out_source(m, h), outs[m].at[:, lanes(g)],
+            out_send.at[m, j], out_recv.at[m, j], z * u + h, p,
+        )
+
+    def out_own(m):
+        return pltpu.make_async_copy(
+            out_source(m, g), outs[m].at[:, lanes(g)], out_recv.at[m, 0]
+        )
+
+    for c in range(chunks):
+        key_tile(z, c, slice(0, (c + 1) * width), True)
+
+    for j in range(1, tp):
+        there = dqpair.at[lax.rem(p + tp - j, tp)]
+        pltpu.make_async_copy(there, there, pair_recv.at[j]).wait()
+    both = jnp.concatenate([dqpair[t] for t in range(tp)], axis=1)
+
+    def w_copy(o, t):
+        return remote(
+            wsend.at[o, t], wrecv.at[me], w_send.at[o, t], w_recv.at[me], p * owners + o, t
+        )
+
+    def w_send_out(o):
+        for t in range(tp):
+            mine = jnp.logical_and(p * owners + o == me, p == t)
+
+            @pl.when(mine)
+            def _():
+                pltpu.make_async_copy(wsend.at[o, t], wrecv.at[me], w_recv.at[me]).start()
+
+            @pl.when(jnp.logical_not(mine))
+            def _():
+                w_copy(o, t).start()
+
+    for o in range(owners):
+        block = dot_first(xbuf[:, o * fw : (o + 1) * fw], both).astype(BF16)
+        for t in range(tp):
+            wsend[o, t] = block[:, t * hd : (t + 1) * hd]
+        if o:
+            w_send_out(o - 1)
+    for j in range(1, u):
+        out_copy(0, j).start()
+    out_own(0).start()
+    w_send_out(owners - 1)
+
+    @pl.loop(1, r - z)
+    def _(k):
+        for j in range(u):
+            wait_stat(-k, j)
+            wait_main(2, k, j)
+            wait_main(3, k, j)
+        for c in range(chunks):
+            key_tile(z + k, c, slice(0, length), False)
+
+    dkv[0] = (acc[1] * scale).astype(BF16)
+    dkv[1] = acc[2].astype(BF16)
+
+    for i in range(sp):
+        pltpu.make_async_copy(wrecv.at[i], wrecv.at[i], w_recv.at[i]).wait()
+    for m in (1, 2):
+        for j in range(1, u):
+            out_copy(m, j).start()
+        out_own(m).start()
+    for h in range(u):
+        total = wrecv[h].astype(F32)
+        for layer in range(1, r):
+            total += wrecv[layer * u + h].astype(F32)
+        w_out[:, h * hd : (h + 1) * hd] = total
+
+    each_send(lambda copy: copy.wait_send())
+    for j in range(1, tp):
+        pair_copy(j).wait_send()
+    for o in range(owners):
+        for t in range(tp):
+
+            @pl.when(jnp.logical_not(jnp.logical_and(p * owners + o == me, p == t)))
+            def _():
+                w_copy(o, t).wait_send()
+
+    for m in range(3):
+        for j in range(u):
+            here = outs[m].at[:, lanes(source_of(j))]
+            pltpu.make_async_copy(here, here, out_recv.at[m, j]).wait()
+            if j:
+                out_copy(m, j).wait_send()
+
+
+def fused_device(sp, tp, *arrays):
+    n, row_width = arrays[0].shape
+    u = arrays[3].shape[1]
+    hd = row_width // u
+    r = sp // u
+    length = u * n
+    features = arrays[7].shape[1]
+    owners = sp // tp
+    fw = features // owners
+    vmem = pl.BlockSpec(memory_space=pltpu.VMEM)
+    dma = pltpu.SemaphoreType.DMA
+    narrow = jax.ShapeDtypeStruct((n, row_width), BF16)
+    return pl.pallas_call(
+        functools.partial(fused_kernel, sp, tp, u, n, hd),
+        out_shape=(narrow, narrow, narrow, jax.ShapeDtypeStruct((fw, row_width), F32)),
+        in_specs=[vmem] * 8,
+        out_specs=(vmem,) * 4,
+        scratch_shapes=[
+            pltpu.VMEM((r, length, hd), BF16),
+            pltpu.VMEM((r, length, hd), BF16),
+            pltpu.VMEM((r, length, hd), BF16),
+            pltpu.VMEM((r, length, hd), BF16),
+            pltpu.VMEM((sp, 8, n), F32),
+            pltpu.VMEM((u, 8, n), F32),
+            pltpu.VMEM((2, n, hd), F32),
+            pltpu.VMEM((3, length, hd), F32),
+            pltpu.VMEM((length, features), BF16),
+            pltpu.VMEM((tp, length, hd), BF16),
+            pltpu.VMEM((2, length, hd), BF16),
+            pltpu.VMEM((3, length, hd), F32),
+            pltpu.VMEM((owners, tp, fw, hd), BF16),
+            pltpu.VMEM((sp, fw, hd), BF16),
+            dma((4, r, u)), dma((4, r, u)),
+            dma((2 * r - 1, u)), dma((2 * r - 1, u)),
+            dma((u,)), dma((u,)),
+            dma((tp,)), dma((tp,)),
+            dma((3, u)), dma((3, u)),
+            dma((owners, tp)), dma((sp,)),
+        ],
+        compiler_params=pltpu.CompilerParams(
+            collective_id=0, has_side_effects=True, vmem_limit_bytes=48 * 1024 * 1024
+        ),
+    )(*arrays)
+
+
+def fits(sp, tp, heads, n, hd):
+    return heads > 1 and sp % heads == 0 and sp % tp == 0 and n == hd
+
+
 def solution(mesh):
+    sp, tp = mesh.shape["sp"], mesh.shape["tp"]
+
+    def per_device(*arrays):
+        heads = arrays[3].shape[1]
+        n, row_width = arrays[0].shape
+        if fits(sp, tp, heads, n, row_width // heads):
+            return fused_device(sp, tp, *arrays)
+        return gathered_device(*arrays)
+
     return jax.shard_map(
         per_device,
         mesh=mesh,

time: 342 us -> 63.9 us (0.19)
  blocking collectives: 126 us -> 0 us
  waiting for transfers between devices: 95.7 us -> 0 us
  Pallas kernels: 0 us -> 54.8 us
  local copies, waits for them, and re-layouts: 49.3 us -> 8.18 us
  matrix products: 20.9 us -> 0 us
  starting transfers between devices: 15.4 us -> 0 us
  between operations: 13.9 us -> 0.67 us
  loops' own time: 12.9 us -> 0 us
  other arithmetic: 5.65 us -> 0 us
    all_gather x4 -> x0, blocking collectives: 126 us -> none  [the longest x1 47.5 us: per_device(): lax.all_gather(row_logsums, 'sp', axis=0, tiled=True)]
    all_gather x5 -> x0, waiting for transfers between devices: 93.1 us -> none  [the longest x1 58 us: per_device(): lax.all_gather(value_heads, 'sp', axis=0, tiled=True)]
    pallas_call x0 -> x1, Pallas kernels: none -> 54.8 us  [fused_device(): pl.pallas_call(functools.partial(fused_kernel, sp, tp, u, n, hd), out_sha...]
    dot_general x9 -> x0, matrix products: 20.9 us -> none  [the longest x3 7.31 us: attention_weights(): jnp.einsum('ahd,bhd->hab', query_part, key_part, preferred_element_type=j...]
    while x8 -> x0, local copies, waits for them, and re-layouts: 17.7 us -> none  [over_blocks(): lax.scan(visit_one, running, (jnp.arange(number, dtype=jnp.int32), stacked))]
    all_to_all x1 -> x0, starting transfers between devices: 15.2 us -> none  [per_device(): lax.all_to_all(whole_input, 'sp', split_axis=1, concat_axis=0, tiled=True)]
    another operation x6 -> x0, loops' own time: 12.9 us -> none  [the longest x2 7.25 us: over_blocks(): lax.scan(visit_one, running, (jnp.arange(number, dtype=jnp.int32), stacked))]
    dynamic_slice x7 -> x0, local copies, waits for them, and re-layouts: 12 us -> none  [over_blocks(): lax.scan(visit_one, running, (jnp.arange(number, dtype=jnp.int32), stacked))]
  transfers between devices with their start and end apart: 6 -> 0, of which waited for: 3 -> 0; matrix products, arithmetic and copies ran while one was open for 21% -> 0% of each run, Pallas kernels for 0% -> 0%
where the time goes in v1:
time: 63.9 us; the launch traced here: 63.7 us
  Pallas kernels  54.8 us (86%)
  local copies, waits for them, and re-layouts  8.18 us (13%)
  between operations  0.67 us (1%)
    pallas_call x1, Pallas kernels, fused_device(): pl.pallas_call(functools.partial(fused_kernel, sp, tp, u, n, hd), out_sha...  54.8 us
    unnamed x20, local copies, waits for them, and re-layouts  8.18 us

profile of v1, /device:TPU:8, one launch (start us, length us, event | category | flops | bytes accessed | tf_op | source)
XLA Modules:
  0.0 63.7 jit_solution(10157944984169748566)
XLA Ops:
  0.6 0.0 copy-start.6
  0.6 0.0 copy-start.1
  0.7 0.8 %copy.12.g_ref = f32[128,4]{1,0:T(8,128)S(1)} copy(f32[128,4]{0,1:T(4,128)} %param.11) | data formatting | bytes 4096 | tf_op args[3]
  1.5 0.0 copy-done.6
  1.5 0.1 copy.13.l_ref
  1.6 0.0 copy-done.1
  1.6 0.0 copy-start
  1.6 0.9 %copy-done = bf16[128,1024]{1,0:T(8,128)(2,1)S(1)} copy-done((bf16[128,1024]{1,0:T(8,128)(2,1)S(1)}, bf16[128,1024]{1,0:T(8,128)(2,1)}, u32[]{:S(2)}) %copy-start) | copy-done | bytes 262168
  2.6 0.0 copy-start.2
  2.6 0.9 %copy-done.2 = bf16[128,512]{1,0:T(8,128)(2,1)S(1)} copy-done((bf16[128,512]{1,0:T(8,128)(2,1)S(1)}, bf16[128,512]{1,0:T(8,128)(2,1)}, u32[]{:S(2)}) %copy-start.2) | copy-done | bytes 131096
  3.5 0.0 copy-start.3
  3.5 0.9 %copy-done.3 = bf16[128,512]{1,0:T(8,128)(2,1)S(1)} copy-done((bf16[128,512]{1,0:T(8,128)(2,1)S(1)}, bf16[128,512]{1,0:T(8,128)(2,1)}, u32[]{:S(2)}) %copy-start.3) | copy-done | bytes 131096
  4.4 0.0 copy-start.4
  4.4 0.9 %copy-done.4 = bf16[128,512]{1,0:T(8,128)(2,1)S(1)} copy-done((bf16[128,512]{1,0:T(8,128)(2,1)S(1)}, bf16[128,512]{1,0:T(8,128)(2,1)}, u32[]{:S(2)}) %copy-start.4) | copy-done | bytes 131096
  5.3 0.0 copy-start.5
  5.3 0.9 %copy-done.5 = bf16[128,512]{1,0:T(8,128)(2,1)S(1)} copy-done((bf16[128,512]{1,0:T(8,128)(2,1)S(1)}, bf16[128,512]{1,0:T(8,128)(2,1)}, u32[]{:S(2)}) %copy-start.5) | copy-done | bytes 131096
  6.2 54.8 %shard_map.111 = (bf16[128,512]{1,0:T(8,128)(2,1)S(1)}, bf16[128,512]{1,0:T(8,128)(2,1)S(1)}, bf16[128,512]{1,0:T(8,128)(2,1)S(1)}, f32[128,512]{1,0:T(8,128)S(1)}) custom-call(bf16[128,512]{1,0:T(8,128)(2,1)S(1)} %copy-done.1, bf16[128,512]{1,0:T(8,128)(2,1)S(1)} %copy-done.2, bf16[128,512]{1,0:T(8,128)(2,1)S(1)} %copy-done.3, f32[128,4]{1,0:T(8,128)S(1)} %copy.12.g_ref, ...), custom_call_target="tpu_custom_call" | custom-call | tf_op jit(solution)/shard_map/pallas_call | solution.py:523
  61.0 0.7 %copy.18 = bf16[128,512]{1,0:T(8,128)(2,1)} copy(bf16[128,512]{1,0:T(8,128)(2,1)S(1)} %get-tuple-element.8) | data formatting | bytes 262144
  61.6 0.7 %copy.19 = bf16[128,512]{1,0:T(8,128)(2,1)} copy(bf16[128,512]{1,0:T(8,128)(2,1)S(1)} %get-tuple-element.9) | data formatting | bytes 262144
  62.3 0.7 %copy.20 = bf16[128,512]{1,0:T(8,128)(2,1)} copy(bf16[128,512]{1,0:T(8,128)(2,1)S(1)} %get-tuple-element.10) | data formatting | bytes 262144
  63.0 0.7 %copy.21 = f32[128,512]{1,0:T(8,128)} copy(f32[128,512]{1,0:T(8,128)S(1)} %get-tuple-element.11) | data formatting | bytes 524288
Async XLA Ops:
  0.6 0.8 %copy-start.6 = (f32[128,4]{0,1:T(4,128)S(1)}, f32[128,4]{0,1:T(4,128)}, u32[]{:S(2)}) copy-start(f32[128,4]{0,1:T(4,128)} %param.12) | copy-start | bytes 6148
  0.6 1.0 %copy-start.1 = (bf16[128,512]{1,0:T(8,128)(2,1)S(1)}, bf16[128,512]{1,0:T(8,128)(2,1)}, u32[]{:S(2)}) copy-start(bf16[128,512]{1,0:T(8,128)(2,1)} %q_ref.1) | copy-start | bytes 393220
  1.6 1.0 %copy-start = (bf16[128,1024]{1,0:T(8,128)(2,1)S(1)}, bf16[128,1024]{1,0:T(8,128)(2,1)}, u32[]{:S(2)}) copy-start(bf16[128,1024]{1,0:T(8,128)(2,1)} %x_ref.1) | copy-start | bytes 786436
  2.6 0.9 %copy-start.2 = (bf16[128,512]{1,0:T(8,128)(2,1)S(1)}, bf16[128,512]{1,0:T(8,128)(2,1)}, u32[]{:S(2)}) copy-start(bf16[128,512]{1,0:T(8,128)(2,1)} %k_ref.1) | copy-start | bytes 393220
  3.5 0.9 %copy-start.3 = (bf16[128,512]{1,0:T(8,128)(2,1)S(1)}, bf16[128,512]{1,0:T(8,128)(2,1)}, u32[]{:S(2)}) copy-start(bf16[128,512]{1,0:T(8,128)(2,1)} %v_ref.1) | copy-start | bytes 393220
  4.4 0.9 %copy-start.4 = (bf16[128,512]{1,0:T(8,128)(2,1)S(1)}, bf16[128,512]{1,0:T(8,128)(2,1)}, u32[]{:S(2)}) copy-start(bf16[128,512]{1,0:T(8,128)(2,1)} %o_ref.1) | copy-start | bytes 393220
  5.3 0.9 %copy-start.5 = (bf16[128,512]{1,0:T(8,128)(2,1)S(1)}, bf16[128,512]{1,0:T(8,128)(2,1)}, u32[]{:S(2)}) copy-start(bf16[128,512]{1,0:T(8,128)(2,1)} %do_ref.1) | copy-start | bytes 393220

commit v2 on v1

--- a/solution.py
+++ b/solution.py
@@ -209,11 +209,11 @@
 
 def fused_kernel(
     sp, tp, u, n, hd,
-    q_ref, k_ref, v_ref, g_ref, l_ref, o_ref, do_ref, x_ref,
-    dq_out, dk_out, dv_out, w_out,
-    kbuf, vbuf, qbuf, dobuf, sbuf, ssend, tmp, cols, xbuf, dqpair, dkv, acc, wsend, wrecv,
+    q_hbm, k_hbm, v_hbm, g_ref, l_ref, o_hbm, do_hbm, x_ref,
+    dq_out, dk_out, dv_out, wrecv,
+    held, kbuf, vbuf, qbuf, dobuf, sbuf, ssend, cols, xbuf, dqpair, dkv, acc, wsend,
     main_send, main_recv, stat_send, stat_recv, x_send, x_recv,
-    pair_send, pair_recv, out_send, out_recv, w_send, w_recv,
+    pair_send, pair_recv, out_send, out_recv, w_send, w_recv, load_sem, relay_send,
 ):
     r = sp // u
     length = u * n
@@ -235,6 +235,11 @@
             device_id={"sp": i, "tp": t}, device_id_type=pl.DeviceIdType.MESH,
         )
 
+    operands = (o_hbm, do_hbm, q_hbm, k_hbm, v_hbm)
+    loads = [pltpu.make_async_copy(ref, held.at[i], load_sem.at[i]) for i, ref in enumerate(operands)]
+    for load in loads:
+        load.start()
+    o_ref, do_ref, q_ref, k_ref, v_ref = (held.at[i] for i in range(5))
     barrier = pltpu.get_barrier_semaphore()
     for d in range(1, sp * tp):
         other = lax.rem(me * tp + p + d, sp * tp)
@@ -243,6 +248,8 @@
             device_id_type=pl.DeviceIdType.MESH,
         )
 
+    loads[0].wait()
+    loads[1].wait()
     lane = lax.broadcasted_iota(jnp.int32, (n, hd), 1)
     terms = jnp.zeros((n, hd), F32)
     for h in range(u):
@@ -251,14 +258,12 @@
             o_ref[:, part].astype(F32) * do_ref[:, part].astype(F32), axis=1, keepdims=True
         )
         terms = jnp.where(lane == h, total, terms)
-    tmp[0] = jnp.zeros((n, hd), F32)
-    tmp[1] = jnp.zeros((n, hd), F32)
-    tmp[0, :, 0:u] = g_ref[...]
-    tmp[1, :, 0:u] = g_ref[...] - l_ref[...]
-    flat = (tmp[0].T, tmp[1].T, terms.T)
+    flat = (g_ref[...], g_ref[...] - l_ref[...], terms.T)
     for h in range(u):
         for s in range(3):
             ssend[h, s : s + 1, :] = flat[s][h : h + 1, :]
+    for load in loads[2:]:
+        load.wait()
     pl.semaphore_wait(barrier, sp * tp - 1)
 
     def head_of(j):
@@ -315,13 +320,31 @@
     def down(k):
         return z >= k
 
+    def relay(a, k):
+        buf = pairs[a][1]
+        layer, step = (z - k, 1) if a < 2 else (z + k, -1)
+        return remote(
+            buf.at[layer], buf.at[layer], relay_send.at[a, k], main_recv.at[a, k + 1, 0],
+            (z + step) * u + g, p,
+        )
+
+    def wait_layer(a, k):
+        if k < 3:
+            for j in range(u):
+                wait_main(a, k, j)
+        else:
+            here = pairs[a][1].at[z - k if a < 2 else z + k]
+            pltpu.make_async_copy(here, here, main_recv.at[a, k, 0]).wait()
+
+    order = [k for k in (2, 1) if k < r] + list(range(3, r))
+
     def each_send(act):
         for j in range(1, u):
             act(stat_copy(0, j))
         for a in (2, 0, 3, 1):
             for j in range(1, u):
                 act(main_copy(a, 0, j))
-        for k in range(1, r):
+        for k in order:
             for reach, sign, members in ((up, 1, (0, 1)), (down, -1, (2, 3))):
 
                 @pl.when(reach(k))
@@ -330,7 +353,8 @@
                         act(stat_copy(sign * k, j))
                     for a in members:
                         for j in range(u):
-                            act(main_copy(a, k, j))
+                            if k < 3:
+                                act(main_copy(a, k, j))
 
         for j in range(1, u):
             act(x_copy(j))
@@ -391,14 +415,47 @@
     for c in range(chunks):
         query_tile(z, c, slice(c * width, length), True)
 
-    @pl.loop(1, z + 1)
-    def _(k):
-        for j in range(u):
-            wait_stat(k, j)
-            wait_main(0, k, j)
-            wait_main(1, k, j)
-        for c in range(chunks):
-            query_tile(z - k, c, slice(0, length), False)
+    def passes(k):
+        far = 2 <= k < r - 1
+        return (jnp.logical_and(down(k), z + 1 < r) if far else None,
+                jnp.logical_and(up(k), z >= 1) if far else None)
+
+    for k in order:
+        onward, back = passes(k)
+        if back is not None:
+
+            @pl.when(back)
+            def _():
+                wait_layer(2, k)
+                relay(2, k).start()
+                wait_layer(3, k)
+                relay(3, k).start()
+
+        if onward is not None:
+
+            @pl.when(onward)
+            def _():
+                wait_layer(0, k)
+                relay(0, k).start()
+                wait_layer(1, k)
+                relay(1, k).start()
+
+        @pl.when(down(k))
+        def _():
+            for j in range(u):
+                wait_stat(k, j)
+            if onward is None:
+                wait_layer(0, k)
+                wait_layer(1, k)
+            else:
+
+                @pl.when(jnp.logical_not(onward))
+                def _():
+                    wait_layer(0, k)
+                    wait_layer(1, k)
+
+            for c in range(chunks):
+                query_tile(z - k, c, slice(0, length), False)
 
     dqpair[p] = (acc[0] * scale).astype(BF16)
     for j in range(u):
@@ -466,33 +523,48 @@
     out_own(0).start()
     w_send_out(owners - 1)
 
-    @pl.loop(1, r - z)
-    def _(k):
-        for j in range(u):
-            wait_stat(-k, j)
-            wait_main(2, k, j)
-            wait_main(3, k, j)
-        for c in range(chunks):
-            key_tile(z + k, c, slice(0, length), False)
+    for k in order:
+        back = passes(k)[1]
+
+        @pl.when(up(k))
+        def _():
+            for j in range(u):
+                wait_stat(-k, j)
+            if back is None:
+                wait_layer(2, k)
+                wait_layer(3, k)
+            else:
+
+                @pl.when(jnp.logical_not(back))
+                def _():
+                    wait_layer(2, k)
+                    wait_layer(3, k)
+
+            for c in range(chunks):
+                key_tile(z + k, c, slice(0, length), False)
 
     dkv[0] = (acc[1] * scale).astype(BF16)
     dkv[1] = acc[2].astype(BF16)
 
-    for i in range(sp):
-        pltpu.make_async_copy(wrecv.at[i], wrecv.at[i], w_recv.at[i]).wait()
+    each_send(lambda copy: copy.wait_send())
+    for j in range(1, tp):
+        pair_copy(j).wait_send()
+    for k in order:
+        onward, back = passes(k)
+        for gate, members in ((onward, (0, 1)), (back, (2, 3))):
+            if gate is not None:
+
+                @pl.when(gate)
+                def _():
+                    for a in members:
+                        relay(a, k).wait_send()
+
     for m in (1, 2):
         for j in range(1, u):
             out_copy(m, j).start()
         out_own(m).start()
-    for h in range(u):
-        total = wrecv[h].astype(F32)
-        for layer in range(1, r):
-            total += wrecv[layer * u + h].astype(F32)
-        w_out[:, h * hd : (h + 1) * hd] = total
-
-    each_send(lambda copy: copy.wait_send())
-    for j in range(1, tp):
-        pair_copy(j).wait_send()
+    for i in range(sp):
+        pltpu.make_async_copy(wrecv.at[i], wrecv.at[i], w_recv.at[i]).wait()
     for o in range(owners):
         for t in range(tp):
 
@@ -506,6 +578,25 @@
             pltpu.make_async_copy(here, here, out_recv.at[m, j]).wait()
             if j:
                 out_copy(m, j).wait_send()
+
+
+def finish_kernel(sp, u, hd, dq, dk, dv, parts, dq_out, dk_out, dv_out, w_out, total, sems):
+    copies = [
+        pltpu.make_async_copy(src, dst, sems.at[i])
+        for i, (src, dst) in enumerate(
+            ((dq, dq_out), (dk, dk_out), (dv, dv_out), (total, w_out))
+        )
+    ]
+    for copy in copies[:3]:
+        copy.start()
+    for h in range(u):
+        running = parts[h].astype(F32)
+        for i in range(h + u, sp, u):
+            running += parts[i].astype(F32)
+        total[:, h * hd : (h + 1) * hd] = running
+    copies[3].start()
+    for copy in copies:
+        copy.wait()
 
 
 def fused_device(sp, tp, *arrays):
@@ -518,39 +609,46 @@
     owners = sp // tp
     fw = features // owners
     vmem = pl.BlockSpec(memory_space=pltpu.VMEM)
+    hbm = pl.BlockSpec(memory_space=pl.ANY)
     dma = pltpu.SemaphoreType.DMA
     narrow = jax.ShapeDtypeStruct((n, row_width), BF16)
-    return pl.pallas_call(
+    parts = pl.pallas_call(
         functools.partial(fused_kernel, sp, tp, u, n, hd),
-        out_shape=(narrow, narrow, narrow, jax.ShapeDtypeStruct((fw, row_width), F32)),
-        in_specs=[vmem] * 8,
+        out_shape=(narrow, narrow, narrow, jax.ShapeDtypeStruct((sp, fw, hd), BF16)),
+        in_specs=[hbm, hbm, hbm, vmem, vmem, hbm, hbm, hbm],
         out_specs=(vmem,) * 4,
         scratch_shapes=[
+            pltpu.VMEM((5, n, row_width), BF16),
             pltpu.VMEM((r, length, hd), BF16),
             pltpu.VMEM((r, length, hd), BF16),
             pltpu.VMEM((r, length, hd), BF16),
             pltpu.VMEM((r, length, hd), BF16),
             pltpu.VMEM((sp, 8, n), F32),
             pltpu.VMEM((u, 8, n), F32),
-            pltpu.VMEM((2, n, hd), F32),
             pltpu.VMEM((3, length, hd), F32),
             pltpu.VMEM((length, features), BF16),
             pltpu.VMEM((tp, length, hd), BF16),
             pltpu.VMEM((2, length, hd), BF16),
             pltpu.VMEM((3, length, hd), F32),
             pltpu.VMEM((owners, tp, fw, hd), BF16),
-            pltpu.VMEM((sp, fw, hd), BF16),
             dma((4, r, u)), dma((4, r, u)),
             dma((2 * r - 1, u)), dma((2 * r - 1, u)),
             dma((u,)), dma((u,)),
             dma((tp,)), dma((tp,)),
             dma((3, u)), dma((3, u)),
-            dma((owners, tp)), dma((sp,)),
+            dma((owners, tp)), dma((sp,)), dma((5,)), dma((4, r)),
         ],
         compiler_params=pltpu.CompilerParams(
-            collective_id=0, has_side_effects=True, vmem_limit_bytes=48 * 1024 * 1024
+            collective_id=0, has_side_effects=True
         ),
-    )(*arrays)
+    )(*arrays[:3], arrays[3].T, arrays[4].T, *arrays[5:])
+    return pl.pallas_call(
+        functools.partial(finish_kernel, sp, u, hd),
+        out_shape=(narrow, narrow, narrow, jax.ShapeDtypeStruct((fw, row_width), F32)),
+        in_specs=[vmem] * 4,
+        out_specs=(hbm,) * 4,
+        scratch_shapes=[pltpu.VMEM((fw, row_width), F32), dma((4,))],
+    )(*parts)
 
 
 def fits(sp, tp, heads, n, hd):

time: 63.9 us -> 53.9 us (0.84)
  local copies, waits for them, and re-layouts: 8.18 us -> 0 us
  Pallas kernels: 54.8 us -> 53.1 us
    unnamed x20 -> x0, local copies, waits for them, and re-layouts: 8.18 us -> none
    pallas_call x1, Pallas kernels: 54.8 us -> 50.9 us  [fused_device(): pl.pallas_call(functools.partial(fused_kernel, sp, tp, u, n, hd), out_sha...]
    pallas_call x0 -> x1, Pallas kernels: none -> 2.11 us  [fused_device(): pl.pallas_call(functools.partial(finish_kernel, sp, u, hd), out_shape=(na...]
where the time goes in v2:
time: 53.9 us; the launch traced here: 53.7 us
  Pallas kernels  53.1 us (99%)
  between operations  0.64 us (1%)
    pallas_call x1, Pallas kernels, fused_device(): pl.pallas_call(functools.partial(fused_kernel, sp, tp, u, n, hd), out_sha...  50.9 us
    pallas_call x1, Pallas kernels, fused_device(): pl.pallas_call(functools.partial(finish_kernel, sp, u, hd), out_shape=(na...  2.11 us

profile of v2, /device:TPU:8, one launch (start us, length us, event | category | flops | bytes accessed | tf_op | source)
XLA Modules:
  0.0 53.7 jit_solution(801188765725736799)
XLA Ops:
  0.6 50.9 %shard_map.111 = (bf16[128,512]{1,0:T(8,128)(2,1)}, bf16[128,512]{1,0:T(8,128)(2,1)}, bf16[128,512]{1,0:T(8,128)(2,1)}, bf16[16,128,128]{2,1,0:T(8,128)(2,1)}) custom-call(bf16[128,512]{1,0:T(8,128)(2,1)} %q_hbm.1, bf16[128,512]{1,0:T(8,128)(2,1)} %k_hbm.1, bf16[128,512]{1,0:T(8,128)(2,1)} %v_hbm.1, f32[4,128]{1,0:T(4,128)} %bitcast.2, f32[4,128]{1,0:T(4,128)} %bitcast.3, ...), custom_call_target="tpu_custom_call" | custom-call | tf_op jit(solution)/shard_map/pallas_call | solution.py:615
  51.6 2.1 %shard_map.112 = (bf16[128,512]{1,0:T(8,128)(2,1)}, bf16[128,512]{1,0:T(8,128)(2,1)}, bf16[128,512]{1,0:T(8,128)(2,1)}, f32[128,512]{1,0:T(8,128)}) custom-call(bf16[128,512]{1,0:T(8,128)(2,1)} %get-tuple-element.8.dq, bf16[128,512]{1,0:T(8,128)(2,1)} %get-tuple-element.9.dk, bf16[128,512]{1,0:T(8,128)(2,1)} %get-tuple-element.10.dv, ...), custom_call_target="tpu_custom_call" | custom-call | tf_op jit(solution)/shard_map/pallas_call | solution.py:645
